TPU v7x, 32 devices: a whole 2x2x4 slice. The times are simulated.
32 devices in a mesh: sp: 8 (over z, x), tp: 4 (over y, core).
Axes of the slice: x: 2, y: 2, z: 4, core: 2. Of those that a mesh axis runs over, the one named last changes fastest.
Arguments:
- resid: bfloat16 [6144, 2048], P(('sp', 'tp')), may hold values from -6 to 6
- queries: bfloat16 [6144, 1024], P('sp', 'tp'), may hold values from -160 to 160
- keys: bfloat16 [6144, 1024], P('sp', 'tp'), may hold values from -6 to 6
- values: bfloat16 [6144, 1024], P('sp', 'tp'), may hold values from -6 to 6
- cum_gate: float32 [6144, 16], P('sp', 'tp'), may hold values from -694 to 0, as said below
- out_weight: bfloat16 [1024, 2048], P('tp'), may hold values from -0.375 to 0.375
- norm_gain: float32 [2048], replicated, may hold values from 0.1 to 1.9
- gate_weight: bfloat16 [2048, 5504], P('sp', 'tp'), may hold values from -0.125 to 0.125
- up_weight: bfloat16 [2048, 5504], P('sp', 'tp'), may hold values from -0.125 to 0.125
- down_weight: bfloat16 [5504, 2048], P('tp', 'sp'), may hold values from -0.078125 to 0.078125
Outputs:
- layer_out: bfloat16 [6144, 2048], P(('sp', 'tp'))
Inputs may be any that keep to these rules, and one draw needn't show every extreme that they name: `cum_gate`: each column is non-increasing along positions and starts at or below zero.
All inputs are finite; a program needn't handle non-finite values.
Results may differ from a plain program's by a relative error of at most 0.01.
Values may be sent and summed in bfloat16 or wider, within the bound.
No kernel may reach another device: no remote copies, remote signals or barrier semaphores. Data moves between devices by JAX's collectives and lax.ppermute only.
A program may use at most 256 MiB of HBM per device.

v0:
```python
import jax
import jax.numpy as jnp
from jax import lax
from jax.sharding import PartitionSpec as P

HEAD_DIM = 64


def rms_norm(mixed, norm_gain):
    scaled = mixed * lax.rsqrt(jnp.mean(mixed * mixed, axis=-1, keepdims=True) + 1e-06) * norm_gain
    return scaled.astype(jnp.bfloat16)


def rounded(term):
    return term.astype(jnp.bfloat16).astype(jnp.float32)


def local(
    resid,
    queries,
    keys,
    values,
    cum_gate,
    out_weight,
    norm_gain,
    gate_weight,
    up_weight,
    down_weight,
):
    rows = queries.shape[0]
    heads_here = cum_gate.shape[1]
    scale = HEAD_DIM ** (-0.5)
    proj_weight = lax.all_gather(out_weight, "tp", axis=0, tiled=True)
    first = lax.axis_index("sp") * rows
    gates_all = lax.all_gather(cum_gate, "sp", axis=0, tiled=True)
    query_heads = queries.reshape(rows, heads_here, HEAD_DIM)
    query_pos = first + jnp.arange(rows, dtype=jnp.int32)
    query_gate = cum_gate.T
    best = jnp.full((heads_here, rows), -1e30, jnp.float32)
    key_piece = lax.all_gather(keys, "sp", axis=0, tiled=True)
    value_piece = lax.all_gather(values, "sp", axis=0, tiled=True)
    count = key_piece.shape[0]
    key_heads = key_piece.reshape(count, heads_here, HEAD_DIM)
    value_heads = value_piece.reshape(count, heads_here, HEAD_DIM)
    key_gate = gates_all.T
    score = (
        jnp.einsum("qhd,khd->hqk", query_heads, key_heads, preferred_element_type=jnp.float32)
        * scale
    )
    score = score + query_gate[:, :, None] - key_gate[:, None, :]
    key_pos = jnp.arange(count, dtype=jnp.int32)
    score = jnp.where(key_pos[None, None, :] <= query_pos[None, :, None], score, -jnp.inf)
    new_best = jnp.maximum(best, jnp.max(score, axis=-1))
    weight = jnp.exp(score - new_best[:, :, None])
    total = jnp.sum(weight, axis=-1)
    numer = jnp.einsum(
        "hqk,khd->hqd", weight.astype(jnp.bfloat16), value_heads, preferred_element_type=jnp.float32
    )
    best, total, numer = (new_best, total, numer)
    attn = (
        (numer / total[:, :, None])
        .transpose(1, 0, 2)
        .reshape(rows, heads_here * HEAD_DIM)
        .astype(jnp.bfloat16)
    )
    groups = lax.axis_size("tp")
    share = rows // groups
    own_rows = lax.all_to_all(attn, "tp", split_axis=0, concat_axis=1, tiled=True)
    group_width = attn.shape[1]
    row_groups = own_rows.reshape(share, groups, group_width)
    weight_groups = proj_weight.reshape(groups, group_width, proj_weight.shape[1])
    terms = jnp.einsum(
        "rgc,gcd->grd", row_groups, weight_groups, preferred_element_type=jnp.float32
    )
    proj = jnp.sum(rounded(terms), axis=0)
    mixed = resid.astype(jnp.float32) + proj
    normed_all = lax.all_gather(rms_norm(mixed, norm_gain), "tp", axis=0, tiled=True)
    gate_sum = jnp.dot(
        normed_all,
        lax.all_gather(gate_weight, "sp", axis=0, tiled=True),
        preferred_element_type=jnp.float32,
    )
    up_sum = jnp.dot(
        normed_all,
        lax.all_gather(up_weight, "sp", axis=0, tiled=True),
        preferred_element_type=jnp.float32,
    )
    hidden = (jax.nn.silu(gate_sum) * up_sum).astype(jnp.bfloat16)
    ffn_part = jnp.dot(
        hidden,
        lax.all_gather(down_weight, "sp", axis=1, tiled=True),
        preferred_element_type=jnp.float32,
    )
    ffn = lax.psum_scatter(
        rounded(ffn_part).astype(jnp.bfloat16), "tp", scatter_dimension=0, tiled=True
    ).astype(jnp.float32)
    return (mixed + 0.5 * ffn).astype(jnp.bfloat16)


def solution(mesh):
    in_specs = (
        P(("sp", "tp"), None),
        P("sp", "tp"),
        P("sp", "tp"),
        P("sp", "tp"),
        P("sp", "tp"),
        P("tp", None),
        P(),
        P("sp", "tp"),
        P("sp", "tp"),
        P("tp", "sp"),
    )
    out_specs = P(("sp", "tp"), None)
    return jax.shard_map(local, mesh=mesh, in_specs=in_specs, out_specs=out_specs, check_vma=False)
```

profile of v0, /device:TPU:0, one launch (start us, length us, event | category | flops | bytes accessed | tf_op | source)
XLA Modules:
  0.0 547.3 jit_solution(295551948475313620)
XLA Ops:
  6.5 0.0 copy-start.2
  6.5 0.0 copy-start.1
  6.5 0.0 all-gather.8.cloned.1.call-start
  6.5 0.7 all-gather.8.cloned.1.call-update
  7.3 0.0 all-gather.10.cloned.1.call-start
  7.3 0.7 all-gather.10.cloned.1.call-update
  8.0 0.0 all-gather.12.cloned.1.call-start
  8.1 0.7 all-gather.12.cloned.1.call-update
  8.7 0.0 all-gather.16.cloned.1.call-start
  8.8 0.5 all-gather.16.cloned.1.call-update
  9.3 0.0 all-gather.14.cloned.1.call-start
  9.4 5.7 %iota_compare_fusion = pred[768,6144]{1,0:T(8,128)(4,1)} fusion(s32[768]{0:T(1024)S(1)} %iota_add_fusion), kind=kLoop, calls=%fused_computation.7 | loop fusion | flops 4718592 | bytes 4721664 | tf_op jit(solution)/shard_map/le | solution.py:52
  15.1 0.0 copy-done.2
  15.1 32.9 %all_gather.25 = f32[6144,4]{0,1:T(4,128)S(1)} all-gather(f32[768,4]{0,1:T(4,128)S(1)} %copy-done.2), channel_id=1, replica_groups=mesh['sp'=8,'tp'=4] {'sp'}, dimensions={0}, use_global_device_ids=true | all-gather | bytes 110592 | tf_op jit(solution)/shard_map/all_gather | solution.py:35
  47.9 0.0 copy-done.1
  48.0 0.9 copy.15
  48.9 23.7 %all-gather.8.cloned.1.call-done = bf16[6144,256]{1,0:T(8,128)(2,1)} async-done(((bf16[768,256]{1,0:T(8,128)(2,1)}), bf16[6144,256]{1,0:T(8,128)(2,1)}) %all-gather.8.cloned.1.call-update) | async-done | bytes 3145744 | tf_op jit(solution)/shard_map/all_gather | solution.py:40
  72.6 3.5 copy.16
  76.2 31.1 %fusion.2 = (f32[4,768]{1,0:T(4,128)S(1)}, f32[4,768,6144]{2,1,0:T(8,128)}) fusion(f32[4,6144]{1,0:T(4,128)S(1)} %bitcast.30, f32[4,768]{1,0:T(4,128)S(1)} %bitcast.34, pred[768,6144]{1,0:T(8,128)(4,1)} %iota_compare_fusion, bf16[768,4,64]{0,2,1:T(8,128)(2,1)} %bitcast.33, bf16[6144,4,64]{0,2,1:T(8,128)(2,1)S(1)} %bitcast.29), kind=kOutput, calls=%fused_computation.4 | convolution fusion | flops 2510287872 | bytes 83877888 | tf_op jit(solution)/shard_map/qhd,khd->hqk/dot_general | solution.py:47
  107.3 26.4 %all-gather.10.cloned.1.call-done = bf16[6144,256]{1,0:T(8,128)(2,1)} async-done(((bf16[768,256]{1,0:T(8,128)(2,1)}), bf16[6144,256]{1,0:T(8,128)(2,1)}) %all-gather.10.cloned.1.call-update) | async-done | bytes 3145744 | tf_op jit(solution)/shard_map/all_gather | solution.py:41
  133.7 3.2 copy.17
  136.8 30.4 %fusion = f32[4,768]{1,0:T(4,128)S(1)} fusion(f32[4,768,6144]{2,1,0:T(8,128)} %get-tuple-element.6, f32[4,768]{1,0:T(4,128)S(1)} %broadcast_maximum_fusion, f32[4,6144]{1,0:T(4,128)S(1)} %bitcast.31, f32[4,768]{1,0:T(4,128)S(1)} %bitcast.35, pred[768,6144]{1,0:T(8,128)(4,1)} %iota_compare_fusion), kind=kLoop, calls=%fused_computation.2 | loop fusion | flops 113243136 | bytes 80351232 | tf_op jit(solution)/shard_map/reduce_sum | solution.py:55
  167.2 31.7 %fusion.12 = bf16[768,4,64]{0,2,1:T(8,128)(2,1)} fusion(bf16[6144,4,64]{0,2,1:T(8,128)(2,1)S(1)} %bitcast.28, f32[4,768,6144]{2,1,0:T(8,128)} %get-tuple-element.6, f32[4,768]{1,0:T(4,128)S(1)} %broadcast_maximum_fusion, f32[4,6144]{1,0:T(4,128)S(1)} %bitcast.32, f32[4,768]{1,0:T(4,128)S(1)} %bitcast.36, pred[768,6144]{1,0:T(8,128)(4,1)} %iota_compare_fusion, ...), kind=kOutput, calls=%fused_computation.18 | convolution fusion | flops 2529558528 | bytes 83890176 | tf_op jit(solution)/shard_map/hqk,khd->hqd/dot_general | solution.py:56
  198.9 1.5 convert_element_type.39
  200.4 0.3 copy.18
  200.7 0.0 copy-start
  200.7 9.9 %all_to_all.13 = bf16[4,192,256]{2,1,0:T(8,128)(2,1)S(1)} all-to-all(bf16[4,192,256]{2,1,0:T(8,128)(2,1)S(1)} %copy.18), channel_id=1, replica_groups=mesh['sp'=8,'tp'=4] {'tp'}, dimensions={0} | all-to-all | bytes 786432 | tf_op jit(solution)/shard_map/all_to_all | solution.py:68
  210.7 0.0 all-gather.12.cloned.1.call-done
  210.7 0.0 copy-start.3
  210.7 3.5 convert_reduce_fusion
  214.1 0.0 copy-done
  214.2 0.3 multiply_reduce_fusion
  214.5 0.0 copy-done.3
  214.5 1.1 multiply_convert_fusion.1
  215.6 0.0 all-gather.14.cloned.1.call-update
  215.6 0.0 all-gather.18.cloned.1.call-start
  215.7 0.5 all-gather.18.cloned.1.call-update
  216.2 0.0 all-gather.20.cloned.1.call-start
  216.3 0.7 all-gather.20.cloned.1.call-update
  217.0 8.7 %reduce-scatter.2.cloned.1.call-start = ((), (), s32[]{:S(2)}) async-start(), calls=%async_computation.9 | async-start | bytes 3932160 | tf_op jit(solution)/shard_map/reduce_scatter | solution.py:94
  225.7 36.2 %all-gather.16.cloned.1.call-done = bf16[2048,1376]{0,1:T(8,128)(2,1)} async-done(((bf16[256,1376]{0,1:T(8,128)(2,1)}), bf16[2048,1376]{0,1:T(8,128)(2,1)}) %all-gather.16.cloned.1.call-update) | async-done | bytes 5636112 | tf_op jit(solution)/shard_map/all_gather | solution.py:80
  261.9 28.1 %all-gather.14.cloned.1.call-done = bf16[768,2048]{1,0:T(8,128)(2,1)} async-done(((bf16[192,2048]{1,0:T(8,128)(2,1)}), bf16[768,2048]{1,0:T(8,128)(2,1)}) %all-gather.14.cloned.1.call-update) | async-done | bytes 3145744 | tf_op jit(solution)/shard_map/all_gather | solution.py:77
  290.0 10.2 %fusion.19 = f32[768,1376]{0,1:T(8,128)} fusion(bf16[768,2048]{1,0:T(8,128)(2,1)} %all-gather.14.cloned.1.call-done, bf16[2048,1376]{0,1:T(8,128)(2,1)} %all-gather.16.cloned.1.call-done), kind=kOutput, calls=%fused_computation.26 | convolution fusion | flops 4328521728 | bytes 13008896 | tf_op jit(solution)/shard_map/dot_general | solution.py:78
  300.2 83.3 %all-gather.18.cloned.1.call-done = bf16[2048,1376]{0,1:T(8,128)(2,1)} async-done(((bf16[256,1376]{0,1:T(8,128)(2,1)}), bf16[2048,1376]{0,1:T(8,128)(2,1)}) %all-gather.18.cloned.1.call-update) | async-done | bytes 5636112 | tf_op jit(solution)/shard_map/all_gather | solution.py:85
  383.5 91.8 %all-gather.20.cloned.1.call-done = bf16[1376,2048]{1,0:T(8,128)(2,1)} async-done(((bf16[1376,256]{1,0:T(8,128)(2,1)}), bf16[1376,2048]{1,0:T(8,128)(2,1)}) %all-gather.20.cloned.1.call-update) | async-done | bytes 5636112 | tf_op jit(solution)/shard_map/all_gather | solution.py:91
  475.3 26.4 %convolution_convert_fusion.1 = bf16[768,2048]{1,0:T(8,128)(2,1)} fusion(bf16[1376,2048]{1,0:T(8,128)(2,1)} %all-gather.20.cloned.1.call-done, f32[768,1376]{0,1:T(8,128)} %fusion.19, bf16[768,2048]{1,0:T(8,128)(2,1)} %all-gather.14.cloned.1.call-done, bf16[2048,1376]{0,1:T(8,128)(2,1)} %all-gather.18.cloned.1.call-done), kind=kOutput, calls=%fused_computation.11 | convolution fusion | flops 8664956928 | bytes 21790720 | tf_op jit(solution)/shard_map/dot_general | solution.py:89
  501.7 0.0 reduce-scatter.2.cloned.1.call-update
  501.7 36.2 %reduce-scatter.2.cloned.1.call-done = bf16[192,2048]{1,0:T(8,128)(2,1)} async-done(((bf16[768,2048]{1,0:T(8,128)(2,1)}), bf16[192,2048]{1,0:T(8,128)(2,1)}) %reduce-scatter.2.cloned.1.call-update) | async-done | bytes 786448 | tf_op jit(solution)/shard_map/reduce_scatter | solution.py:94
  537.9 2.3 add_convert_fusion
  (3 shorter events, 0.0 us)
Async XLA Ops:
  6.5 8.6 %copy-start.2 = (f32[768,4]{0,1:T(4,128)S(1)}, f32[768,4]{0,1:T(4,128)}, u32[]{:S(2)}) copy-start(f32[768,4]{0,1:T(4,128)} %param.14) | copy-start | bytes 36868
  6.5 41.4 %copy-start.1 = (bf16[768,256]{1,0:T(8,128)(2,1)S(1)}, bf16[768,256]{1,0:T(8,128)(2,1)}, u32[]{:S(2)}) copy-start(bf16[768,256]{1,0:T(8,128)(2,1)} %param.11) | copy-start | bytes 1179652
  6.5 66.1 %all-gather.8.cloned.1.call-start = ((), (), s32[]{:S(2)}) async-start(), calls=%async_computation.2 | async-start | bytes 3538944 | tf_op jit(solution)/shard_map/all_gather | solution.py:40
  7.3 126.4 %all-gather.10.cloned.1.call-start = ((), (), s32[]{:S(2)}) async-start(), calls=%async_computation.3 | async-start | bytes 3538944 | tf_op jit(solution)/shard_map/all_gather | solution.py:41
  8.0 202.7 %all-gather.12.cloned.1.call-start = ((), (), s32[]{:S(2)}) async-start(), calls=%async_computation.4 | async-start | bytes 5242880 | tf_op jit(solution)/shard_map/all_gather | solution.py:33
  8.7 253.1 %all-gather.16.cloned.1.call-start = ((), (), s32[]{:S(2)}) async-start(), calls=%async_computation.6 | async-start | bytes 6340608 | tf_op jit(solution)/shard_map/all_gather | solution.py:80
  9.3 280.7 %all-gather.14.cloned.1.call-start = ((), (), s32[]{:S(2)}) async-start(), calls=%async_computation.5 | async-start | bytes 3932160 | tf_op jit(solution)/shard_map/all_gather | solution.py:77
  200.7 13.4 %copy-start = (bf16[192,2048]{1,0:T(8,128)(2,1)S(1)}, bf16[192,2048]{1,0:T(8,128)(2,1)}, u32[]{:S(2)}) copy-start(bf16[192,2048]{1,0:T(8,128)(2,1)} %param.10) | copy-start | bytes 2359300
  210.7 3.8 copy-start.3
  215.6 167.8 %all-gather.18.cloned.1.call-start = ((), (), s32[]{:S(2)}) async-start(), calls=%async_computation.7 | async-start | bytes 6340608 | tf_op jit(solution)/shard_map/all_gather | solution.py:85
  216.2 259.1 %all-gather.20.cloned.1.call-start = ((), (), s32[]{:S(2)}) async-start(), calls=%async_computation.8 | async-start | bytes 6340608 | tf_op jit(solution)/shard_map/all_gather | solution.py:91
  217.0 321.0 %reduce-scatter.2.cloned.1.call-start = ((), (), s32[]{:S(2)}) async-start(), calls=%async_computation.9 | async-start | bytes 3932160 | tf_op jit(solution)/shard_map/reduce_scatter | solution.py:94
Sparse Core Ops, SparseCore 0:
  9.5 63.0 all-gather.7
  74.8 58.8 all-gather.9
  135.2 33.1 all-gather.11
  170.3 91.5 all-gather.15
  263.3 26.6 all-gather.13
  291.9 91.5 all-gather.17
  385.5 89.7 all-gather.19
  501.8 36.0 reduce-scatter.1
where the time goes:
time: 551 us; the launch traced here: 547 us
  waiting for transfers between devices  330 us (60%)
  matrix products  103 us (19%)
  blocking collectives  42.8 us (8%)
  other arithmetic  39.9 us (7%)
  between operations  13.8 us (3%)
  local copies, waits for them, and re-layouts  9.49 us (2%)
  starting transfers between devices  8.97 us (2%)
    all_gather x1, waiting for transfers between devices, local(): lax.all_gather(down_weight, 'sp', axis=1, tiled=True)  91.8 us
    all_gather x1, waiting for transfers between devices, local(): lax.all_gather(up_weight, 'sp', axis=0, tiled=True)  83.3 us
    reduce_scatter x1, waiting for transfers between devices, local(): lax.psum_scatter(rounded(ffn_part).astype(jnp.bfloat16), 'tp', scatter_di...  36.2 us
    all_gather x1, waiting for transfers between devices, local(): lax.all_gather(gate_weight, 'sp', axis=0, tiled=True)  36.2 us
    all_gather x1, blocking collectives, local(): gates_all = lax.all_gather(cum_gate, 'sp', axis=0, tiled=True)  32.9 us
    dot_general x1, matrix products, local(): jnp.einsum('hqk,khd->hqd', weight.astype(jnp.bfloat16), value_heads, pref...  31.7 us
    dot_general x1, matrix products, local(): jnp.einsum('qhd,khd->hqk', query_heads, key_heads, preferred_element_type...  31.1 us
    reduce_sum x1, other arithmetic, local(): total = jnp.sum(weight, axis=-1)  30.4 us
  transfers between devices with their start and end apart: 8, of which 7 were waited for; matrix products, arithmetic and copies ran while one was open for 23% of the time, Pallas kernels for 0%

commit v1 on v0

--- a/solution.py
+++ b/solution.py
@@ -32,12 +32,15 @@
     scale = HEAD_DIM ** (-0.5)
     proj_weight = lax.all_gather(out_weight, "tp", axis=0, tiled=True)
     first = lax.axis_index("sp") * rows
-    gates_all = lax.all_gather(cum_gate, "sp", axis=0, tiled=True)
     query_heads = queries.reshape(rows, heads_here, HEAD_DIM)
     query_pos = first + jnp.arange(rows, dtype=jnp.int32)
     query_gate = cum_gate.T
     best = jnp.full((heads_here, rows), -1e30, jnp.float32)
-    key_piece = lax.all_gather(keys, "sp", axis=0, tiled=True)
+    gates_all, key_piece = jnp.split(
+        lax.all_gather(jnp.concatenate([cum_gate, keys], axis=1), "sp", axis=0, tiled=True),
+        [cum_gate.shape[1]],
+        axis=1,
+    )
     value_piece = lax.all_gather(values, "sp", axis=0, tiled=True)
     count = key_piece.shape[0]
     key_heads = key_piece.reshape(count, heads_here, HEAD_DIM)

time: 551 us -> 628 us (1.14)
  waiting for transfers between devices: 330 us -> 441 us
  blocking collectives: 42.8 us -> 0 us
  local copies, waits for them, and re-layouts: 9.49 us -> 21.3 us
    all_gather x1, waiting for transfers between devices: 23.7 us -> 133 us  [local(): lax.all_gather(jnp.concatenate([cum_gate, keys], axis=1), 'sp', axis=0, t...]
    all_gather x1 -> x0, blocking collectives: 32.9 us -> none  [local(): gates_all = lax.all_gather(cum_gate, 'sp', axis=0, tiled=True)]
    all_gather x1, waiting for transfers between devices: 36.2 us -> 4.82 us  [local(): lax.all_gather(gate_weight, 'sp', axis=0, tiled=True)]
    all_gather x1, waiting for transfers between devices: 26.4 us -> 53 us  [local(): value_piece = lax.all_gather(values, 'sp', axis=0, tiled=True)]
    all_to_all x1 -> x0, blocking collectives: 9.94 us -> none  [local(): lax.all_to_all(attn, 'tp', split_axis=0, concat_axis=1, tiled=True)]
    reduce_scatter x1, starting transfers between devices: 8.74 us -> 0.21 us  [local(): lax.psum_scatter(rounded(ffn_part).astype(jnp.bfloat16), 'tp', scatter_di...]
    split x0 -> x2, local copies, waits for them, and re-layouts: none -> 8.44 us  [local(): jnp.split(lax.all_gather(jnp.concatenate([cum_gate, keys], axis=1), 'sp',...]
    all_to_all x0 -> x1, waiting for transfers between devices: none -> 7.3 us  [local(): lax.all_to_all(attn, 'tp', split_axis=0, concat_axis=1, tiled=True)]
  transfers between devices with their start and end apart: 8 -> 9, of which waited for: 7 -> 8; matrix products, arithmetic and copies ran while one was open for 23% -> 22% of each run, Pallas kernels for 0% -> 0%
where the time goes in v1:
time: 628 us; the launch traced here: 624 us
  waiting for transfers between devices  441 us (70%)
  matrix products  102 us (16%)
  other arithmetic  41.4 us (7%)
  local copies, waits for them, and re-layouts  21.3 us (3%)
  between operations  13.8 us (2%)
    all_gather x1, waiting for transfers between devices, local(): lax.all_gather(jnp.concatenate([cum_gate, keys], axis=1), 'sp', axis=0, t...  133 us
    all_gather x1, waiting for transfers between devices, local(): lax.all_gather(down_weight, 'sp', axis=1, tiled=True)  91.8 us
    all_gather x1, waiting for transfers between devices, local(): lax.all_gather(up_weight, 'sp', axis=0, tiled=True)  83.3 us
    all_gather x1, waiting for transfers between devices, local(): value_piece = lax.all_gather(values, 'sp', axis=0, tiled=True)  53 us
    reduce_scatter x1, waiting for transfers between devices, local(): lax.psum_scatter(rounded(ffn_part).astype(jnp.bfloat16), 'tp', scatter_di...  36.2 us
    dot_general x1, matrix products, local(): jnp.einsum('qhd,khd->hqk', query_heads, key_heads, preferred_element_type...  32.5 us
    dot_general x1, matrix products, local(): jnp.einsum('hqk,khd->hqd', weight.astype(jnp.bfloat16), value_heads, pref...  29.9 us
    reduce_sum x1, other arithmetic, local(): total = jnp.sum(weight, axis=-1)  28.8 us
  transfers between devices with their start and end apart: 9, of which 8 were waited for; matrix products, arithmetic and copies ran while one was open for 22% of the time, Pallas kernels for 0%

profile of v1, /device:TPU:0, one launch (start us, length us, event | category | flops | bytes accessed | tf_op | source)
XLA Modules:
  0.0 623.6 jit_solution(1500317411411300822)
XLA Ops:
  6.5 0.0 all-gather.10.cloned.1.call-start
  6.5 0.7 all-gather.10.cloned.1.call-update
  7.3 0.0 all-gather.8.cloned.1.call-start
  7.3 1.0 convert_element_type.40
  8.4 0.9 copy.18
  9.2 0.0 copy-start.2
  9.3 1.5 pad_maximum_fusion
  10.7 0.0 all-gather.8.cloned.1.call-update
  10.8 0.0 all-gather.12.cloned.1.call-start
  10.8 0.7 all-gather.12.cloned.1.call-update
  11.5 0.0 all-gather.16.cloned.1.call-start
  11.5 0.5 all-gather.16.cloned.1.call-update
  12.1 6.3 %iota_compare_fusion = pred[768,6144]{0,1:T(8,128)(4,1)} fusion(s32[768]{0:T(1024)S(1)} %iota_add_fusion), kind=kLoop, calls=%fused_computation.7 | loop fusion | flops 4718592 | bytes 4721664 | tf_op jit(solution)/shard_map/le | solution.py:55
  18.4 0.0 copy-done.2
  18.4 0.9 copy.20
  19.3 53.0 %all-gather.10.cloned.1.call-done = bf16[6144,256]{1,0:T(8,128)(2,1)} async-done(((bf16[768,256]{1,0:T(8,128)(2,1)}), bf16[6144,256]{1,0:T(8,128)(2,1)}) %all-gather.10.cloned.1.call-update) | async-done | bytes 3145744 | tf_op jit(solution)/shard_map/all_gather | solution.py:44
  72.3 5.2 copy.22
  77.4 133.0 %all-gather.8.cloned.1.call-done = f32[6144,260]{1,0:T(8,128)} async-done(((f32[768,260]{1,0:T(8,128)}), f32[6144,260]{1,0:T(8,128)}) %all-gather.8.cloned.1.call-update) | async-done | bytes 6389776 | tf_op jit(solution)/shard_map/all_gather | solution.py:40
  210.4 2.1 slice_bitcast_fusion
  212.5 1.2 copy.21
  213.7 5.3 split.8
  219.0 0.0 copy-start.3
  219.0 3.1 copy.19
  222.2 0.0 copy-done.3
  222.2 32.5 %fusion.2 = (f32[4,768]{1,0:T(4,128)S(1)}, f32[4,6144,768]{2,1,0:T(8,128)}) fusion(f32[4,6144]{1,0:T(4,128)S(1)} %copy.21, f32[4,768]{1,0:T(4,128)S(1)} %bitcast.41, pred[768,6144]{0,1:T(8,128)(4,1)} %iota_compare_fusion, bf16[6144,4,64]{0,2,1:T(8,128)(2,1)} %bitcast.39, bf16[768,4,64]{0,2,1:T(8,128)(2,1)} %bitcast.40), kind=kOutput, calls=%fused_computation.4 | convolution fusion | flops 2510287872 | bytes 83877888 | tf_op jit(solution)/shard_map/qhd,khd->hqk/dot_general | solution.py:50
  254.7 0.0 copy-start.1
  254.7 28.8 %fusion = f32[4,768]{1,0:T(4,128)S(1)} fusion(f32[4,6144,768]{2,1,0:T(8,128)} %get-tuple-element.6, f32[4,768]{1,0:T(4,128)S(1)} %broadcast_maximum_fusion, f32[4,6144]{1,0:T(4,128)S(1)} %copy.21, f32[4,768]{1,0:T(4,128)S(1)} %bitcast.42, pred[768,6144]{0,1:T(8,128)(4,1)} %iota_compare_fusion), kind=kLoop, calls=%fused_computation.2 | loop fusion | flops 113243136 | bytes 80351232 | tf_op jit(solution)/shard_map/reduce_sum | solution.py:58
  283.5 0.0 copy-done.1
  283.5 29.9 %divide_convert_fusion = bf16[768,4,64]{0,2,1:T(8,128)(2,1)} fusion(f32[768,4]{0,1:T(4,128)S(1)} %bitcast.44, bf16[6144,4,64]{0,2,1:T(8,128)(2,1)S(1)} %bitcast.38, f32[4,6144,768]{2,1,0:T(8,128)} %get-tuple-element.6, f32[4,768]{1,0:T(4,128)S(1)} %broadcast_maximum_fusion, f32[4,6144]{1,0:T(4,128)S(1)} %copy.21, f32[4,768]{1,0:T(4,128)S(1)} %bitcast.43, ...), kind=kOutput, calls=%fused_computation.19 | convolution fusion | flops 2529558528 | bytes 83890176 | tf_op jit(solution)/shard_map/hqk,khd->hqd/dot_general | solution.py:59
  313.4 1.5 convert_element_type.43
  314.9 1.1 copy.24
  316.0 0.0 copy-start
  316.0 3.6 all-to-all-start
  319.6 0.0 all-gather.14.cloned.1.call-start
  319.7 0.0 all-gather.12.cloned.1.call-done
  319.7 7.3 %all-to-all-done = bf16[4,192,256]{2,1,0:T(8,128)(2,1)S(1)} async-done(((bf16[4,192,256]{2,1,0:T(8,128)(2,1)}), bf16[4,192,256]{2,1,0:T(8,128)(2,1)S(1)}, u32[]{:S(2)}, u32[]{:S(2)}) %all-to-all-start) | async-done | bytes 393248 | tf_op jit(solution)/shard_map/all_to_all | solution.py:71
  327.0 0.0 copy-start.4
  327.0 3.3 convert_reduce_fusion
  330.3 0.0 copy-done
  330.3 0.3 multiply_reduce_fusion
  330.6 0.0 copy-done.4
  330.6 1.1 multiply_convert_fusion.1
  331.7 0.0 all-gather.14.cloned.1.call-update
  331.8 0.0 all-gather.18.cloned.1.call-start
  331.8 0.5 all-gather.18.cloned.1.call-update
  332.3 0.0 all-gather.20.cloned.1.call-start
  332.4 0.7 all-gather.20.cloned.1.call-update
  333.1 0.2 reduce-scatter.2.cloned.1.call-start
  333.3 4.8 all-gather.16.cloned.1.call-done
  338.1 28.1 %all-gather.14.cloned.1.call-done = bf16[768,2048]{1,0:T(8,128)(2,1)} async-done(((bf16[192,2048]{1,0:T(8,128)(2,1)}), bf16[768,2048]{1,0:T(8,128)(2,1)}) %all-gather.14.cloned.1.call-update) | async-done | bytes 3145744 | tf_op jit(solution)/shard_map/all_gather | solution.py:80
  366.3 10.2 %fusion.13 = f32[768,1376]{0,1:T(8,128)} fusion(bf16[768,2048]{1,0:T(8,128)(2,1)} %all-gather.14.cloned.1.call-done, bf16[2048,1376]{0,1:T(8,128)(2,1)} %all-gather.16.cloned.1.call-done), kind=kOutput, calls=%fused_computation.27 | convolution fusion | flops 4328521728 | bytes 13008896 | tf_op jit(solution)/shard_map/dot_general | solution.py:81
  376.4 83.3 %all-gather.18.cloned.1.call-done = bf16[2048,1376]{0,1:T(8,128)(2,1)} async-done(((bf16[256,1376]{0,1:T(8,128)(2,1)}), bf16[2048,1376]{0,1:T(8,128)(2,1)}) %all-gather.18.cloned.1.call-update) | async-done | bytes 5636112 | tf_op jit(solution)/shard_map/all_gather | solution.py:88
  459.7 91.8 %all-gather.20.cloned.1.call-done = bf16[1376,2048]{1,0:T(8,128)(2,1)} async-done(((bf16[1376,256]{1,0:T(8,128)(2,1)}), bf16[1376,2048]{1,0:T(8,128)(2,1)}) %all-gather.20.cloned.1.call-update) | async-done | bytes 5636112 | tf_op jit(solution)/shard_map/all_gather | solution.py:94
  551.5 26.4 %convolution_convert_fusion.1 = bf16[768,2048]{1,0:T(8,128)(2,1)} fusion(bf16[1376,2048]{1,0:T(8,128)(2,1)} %all-gather.20.cloned.1.call-done, f32[768,1376]{0,1:T(8,128)} %fusion.13, bf16[768,2048]{1,0:T(8,128)(2,1)} %all-gather.14.cloned.1.call-done, bf16[2048,1376]{0,1:T(8,128)(2,1)} %all-gather.18.cloned.1.call-done), kind=kOutput, calls=%fused_computation.11 | convolution fusion | flops 8664956928 | bytes 21790720 | tf_op jit(solution)/shard_map/dot_general | solution.py:92
  578.0 0.0 reduce-scatter.2.cloned.1.call-update
  578.0 36.2 %reduce-scatter.2.cloned.1.call-done = bf16[192,2048]{1,0:T(8,128)(2,1)} async-done(((bf16[768,2048]{1,0:T(8,128)(2,1)}), bf16[192,2048]{1,0:T(8,128)(2,1)}) %reduce-scatter.2.cloned.1.call-update) | async-done | bytes 786448 | tf_op jit(solution)/shard_map/reduce_scatter | solution.py:97
  614.2 2.3 add_convert_fusion
  (3 shorter events, 0.0 us)
Async XLA Ops:
  6.5 65.7 %all-gather.10.cloned.1.call-start = ((), (), s32[]{:S(2)}) async-start(), calls=%async_computation.3 | async-start | bytes 3538944 | tf_op jit(solution)/shard_map/all_gather | solution.py:44
  7.3 203.1 %all-gather.8.cloned.1.call-start = ((), (), s32[]{:S(2)}) async-start(), calls=%async_computation.2 | async-start | bytes 10616832 | tf_op jit(solution)/shard_map/all_gather | solution.py:40
  9.2 9.1 %copy-start.2 = (bf16[768,256]{1,0:T(8,128)(2,1)S(1)}, bf16[768,256]{1,0:T(8,128)(2,1)}, u32[]{:S(2)}) copy-start(bf16[768,256]{1,0:T(8,128)(2,1)} %param.11) | copy-start | bytes 1179652
  10.8 308.9 %all-gather.12.cloned.1.call-start = ((), (), s32[]{:S(2)}) async-start(), calls=%async_computation.4 | async-start | bytes 5242880 | tf_op jit(solution)/shard_map/all_gather | solution.py:33
  11.5 326.6 %all-gather.16.cloned.1.call-start = ((), (), s32[]{:S(2)}) async-start(), calls=%async_computation.6 | async-start | bytes 6340608 | tf_op jit(solution)/shard_map/all_gather | solution.py:83
  219.0 3.2 copy-start.3
  254.7 28.8 %copy-start.1 = (bf16[6144,256]{0,1:T(8,128)(2,1)S(1)}, bf16[6144,256]{0,1:T(8,128)(2,1)}, u32[]{:S(2)}) copy-start(bf16[6144,256]{0,1:T(8,128)(2,1)} %copy.22) | copy-start | bytes 9437188
  316.0 14.3 %copy-start = (bf16[192,2048]{1,0:T(8,128)(2,1)S(1)}, bf16[192,2048]{1,0:T(8,128)(2,1)}, u32[]{:S(2)}) copy-start(bf16[192,2048]{1,0:T(8,128)(2,1)} %param.10) | copy-start | bytes 2359300
  316.0 11.0 %all-to-all-start = ((bf16[4,192,256]{2,1,0:T(8,128)(2,1)}), bf16[4,192,256]{2,1,0:T(8,128)(2,1)S(1)}, u32[]{:S(2)}, u32[]{:S(2)}) async-start(bf16[4,192,256]{2,1,0:T(8,128)(2,1)} %copy.24), calls=%async_computation | async-start | bytes 786432 | tf_op jit(solution)/shard_map/all_to_all | solution.py:71
  319.6 46.6 %all-gather.14.cloned.1.call-start = ((), (), s32[]{:S(2)}) async-start(), calls=%async_computation.5 | async-start | bytes 3932160 | tf_op jit(solution)/shard_map/all_gather | solution.py:80
  327.0 3.6 copy-start.4
  331.8 128.0 %all-gather.18.cloned.1.call-start = ((), (), s32[]{:S(2)}) async-start(), calls=%async_computation.7 | async-start | bytes 6340608 | tf_op jit(solution)/shard_map/all_gather | solution.py:88
  332.3 219.2 %all-gather.20.cloned.1.call-start = ((), (), s32[]{:S(2)}) async-start(), calls=%async_computation.8 | async-start | bytes 6340608 | tf_op jit(solution)/shard_map/all_gather | solution.py:94
  333.1 281.1 %reduce-scatter.2.cloned.1.call-start = ((), (), s32[]{:S(2)}) async-start(), calls=%async_computation.9 | async-start | bytes 3932160 | tf_op jit(solution)/shard_map/reduce_scatter | solution.py:97
Sparse Core Ops, SparseCore 0:
  9.5 62.7 all-gather.9
  74.5 135.8 all-gather.7
  212.0 32.6 all-gather.11
  246.5 91.5 all-gather.15
  339.5 26.6 all-gather.13
  368.2 91.5 all-gather.17
  461.8 89.7 all-gather.19
  578.1 36.0 reduce-scatter.1
